TPU v7x, 32 devices: a whole 2x2x4 slice. The times are simulated.
32 devices in a mesh: fs: 8 (over z, y), tp: 4 (over x, core).
Axes of the slice: x: 2, y: 2, z: 4, core: 2. Of those that a mesh axis runs over, the one named last changes fastest.
Arguments:
- tokens: bfloat16 [8192, 2048], P('fs', 'tp'), may hold values from -6 to 6
- norm_gain: float32 [2048], P('fs'), may hold values from 0.1 to 1.9
- up_master: float32 [2048, 8192], P('fs', 'tp'), may hold values from -0.125 to 0.125
- down_master: float32 [2048, 8192], P('fs', 'tp'), may hold values from -0.0625 to 0.0625
Outputs:
- up_weights: bfloat16 [2048, 8192], P(None, 'tp')
- down_weights: bfloat16 [8192, 2048], P('tp')
- mlp_out: bfloat16 [8192, 2048], P('fs', 'tp')
All inputs are finite; a program needn't handle non-finite values.
Results may differ from a plain program's by a relative error of at most 0.014.
Values may be sent and summed in bfloat16 or wider, within the bound.
A program may use at most 128 MiB of HBM per device.

v0:
```python
import jax
import jax.numpy as jnp
from jax import lax
from jax.sharding import PartitionSpec as P

norm_floor = 1e-06


def on_device(tokens, norm_gain, up_master, down_master):
    up_local = (norm_gain[:, None] * up_master).astype(jnp.bfloat16)
    down_local = down_master.astype(jnp.bfloat16)
    gathered = lax.all_gather(tokens, "tp", axis=1, tiled=True)
    widened = gathered.astype(jnp.float32)
    normed = (
        widened * lax.rsqrt(jnp.mean(widened * widened, axis=-1, keepdims=True) + norm_floor)
    ).astype(jnp.bfloat16)
    up_whole, down_whole = (
        lax.all_gather(up_local, "fs", axis=0, tiled=True),
        lax.all_gather(down_local, "fs", axis=0, tiled=True),
    )
    preact = jnp.dot(normed, up_whole, preferred_element_type=jnp.float32)
    hidden = jnp.square(jax.nn.relu(preact)).astype(jnp.bfloat16)
    partial_value = jnp.einsum("tf,df->td", hidden, down_whole, preferred_element_type=jnp.float32)
    summed = lax.psum_scatter(
        partial_value.astype(jnp.bfloat16), "tp", scatter_dimension=1, tiled=True
    )
    return (up_whole, jnp.transpose(down_whole), summed)


def solution(mesh):
    in_specs = (P("fs", "tp"), P("fs"), P("fs", "tp"), P("fs", "tp"))
    out_specs = (P(None, "tp"), P("tp", None), P("fs", "tp"))
    return jax.shard_map(
        on_device, mesh=mesh, in_specs=in_specs, out_specs=out_specs, check_vma=False
    )
```

profile of v0, /device:TPU:0, one launch (start us, length us, event | category | flops | bytes accessed | tf_op | source)
XLA Modules:
  0.0 391.6 jit_solution(10137496696475460250)
XLA Ops:
  7.2 0.0 all-gather.8.cloned.1.call-start
  7.2 0.7 all-gather.8.cloned.1.call-update
  7.9 0.0 all-gather.4.cloned.1.call-start
  7.9 2.7 multiply_convert_fusion.1
  10.7 0.0 all-gather.4.cloned.1.call-update
  10.7 0.0 all-gather.6.cloned.1.call-start
  10.8 2.5 copy.7
  13.3 0.0 all-gather.6.cloned.1.call-update
  13.3 0.0 reduce-scatter.2.cloned.1.call-start
  13.4 33.4 %all-gather.8.cloned.1.call-done = bf16[1024,2048]{1,0:T(8,128)(2,1)} async-done(((bf16[1024,512]{1,0:T(8,128)(2,1)}), bf16[1024,2048]{1,0:T(8,128)(2,1)}) %all-gather.8.cloned.1.call-update) | async-done | bytes 4194320 | tf_op jit(solution)/shard_map/all_gather | solution.py:12
  46.7 3.1 fusion
  49.8 124.1 %all-gather.4.cloned.1.call-done = bf16[2048,2048]{1,0:T(8,128)(2,1)} async-done(((bf16[256,2048]{1,0:T(8,128)(2,1)}), bf16[2048,2048]{1,0:T(8,128)(2,1)}) %all-gather.4.cloned.1.call-update) | async-done | bytes 8388624 | tf_op jit(solution)/shard_map/all_gather | solution.py:18
  174.0 125.8 %all-gather.6.cloned.1.call-done = bf16[2048,2048]{0,1:T(8,128)(2,1)} async-done(((bf16[256,2048]{0,1:T(8,128)(2,1)}), bf16[2048,2048]{0,1:T(8,128)(2,1)}) %all-gather.6.cloned.1.call-update) | async-done | bytes 8388624 | tf_op jit(solution)/shard_map/all_gather | solution.py:19
  299.7 25.7 %fusion.9 = bf16[1024,2048]{1,0:T(8,128)(2,1)} fusion(bf16[2048,2048]{0,1:T(8,128)(2,1)} %all-gather.6.cloned.1.call-done, bf16[2048,2048]{1,0:T(8,128)(2,1)} %all-gather.4.cloned.1.call-done, bf16[1024,2048]{1,0:T(8,128)(2,1)} %all-gather.8.cloned.1.call-done, f32[1024]{0:T(1024)S(1)} %add_rsqrt_fusion), kind=kOutput, calls=%fused_computation.8 | convolution fusion | flops 17194549248 | bytes 25169920 | tf_op jit(solution)/shard_map/tf,df->td/dot_general | solution.py:23
  325.4 0.0 reduce-scatter.2.cloned.1.call-update
  325.5 42.7 %reduce-scatter.2.cloned.1.call-done = bf16[1024,512]{1,0:T(8,128)(2,1)} async-done(((bf16[1024,2048]{1,0:T(8,128)(2,1)}), bf16[1024,512]{1,0:T(8,128)(2,1)}) %reduce-scatter.2.cloned.1.call-update) | async-done | bytes 1048592 | tf_op jit(solution)/shard_map/reduce_scatter | solution.py:24
  368.2 8.4 %copy.10 = bf16[2048,2048]{1,0:T(8,128)(2,1)} copy(bf16[2048,2048]{1,0:T(8,128)(2,1)} %all-gather.4.cloned.1.call-done) | data formatting | bytes 16777216
  376.6 8.4 %copy.11 = bf16[2048,2048]{1,0:T(8,128)(2,1)} copy(bf16[2048,2048]{1,0:T(8,128)(2,1)} %bitcast.3) | data formatting | bytes 16777216
  (1 shorter events, 0.0 us)
Async XLA Ops:
  7.2 39.6 %all-gather.8.cloned.1.call-start = ((), (), s32[]{:S(2)}) async-start(), calls=%async_computation.3 | async-start | bytes 5242880 | tf_op jit(solution)/shard_map/all_gather | solution.py:12
  7.9 166.1 %all-gather.4.cloned.1.call-start = ((), (), s32[]{:S(2)}) async-start(), calls=%async_computation.1 | async-start | bytes 9437184 | tf_op jit(solution)/shard_map/all_gather | solution.py:18
  10.7 289.0 %all-gather.6.cloned.1.call-start = ((), (), s32[]{:S(2)}) async-start(), calls=%async_computation.2 | async-start | bytes 9437184 | tf_op jit(solution)/shard_map/all_gather | solution.py:19
  13.3 354.8 %reduce-scatter.2.cloned.1.call-start = ((), (), s32[]{:S(2)}) async-start(), calls=%async_computation.4 | async-start | bytes 5242880 | tf_op jit(solution)/shard_map/reduce_scatter | solution.py:24
Sparse Core Ops, SparseCore 0:
  9.5 37.1 all-gather.7
  49.4 124.4 all-gather.3
  176.6 123.1 all-gather.5
  325.6 42.5 reduce-scatter.1
where the time goes:
time: 392 us
  waiting for transfers between devices  327 us (83%)
  matrix products  25.7 us (7%)
  local copies, waits for them, and re-layouts  19.4 us (5%)
  between operations  13.8 us (4%)
  other arithmetic  5.82 us (1%)
    all_gather x1, waiting for transfers between devices, on_device(): lax.all_gather(down_local, 'fs', axis=0, tiled=True)  126 us
    all_gather x1, waiting for transfers between devices, on_device(): lax.all_gather(up_local, 'fs', axis=0, tiled=True)  124 us
    reduce_scatter x1, waiting for transfers between devices, on_device(): lax.psum_scatter(partial_value.astype(jnp.bfloat16), 'tp', scatter_dimens...  42.7 us
    all_gather x1, waiting for transfers between devices, on_device(): gathered = lax.all_gather(tokens, 'tp', axis=1, tiled=True)  33.4 us
    dot_general x1, matrix products, on_device(): jnp.einsum('tf,df->td', hidden, down_whole, preferred_element_type=jnp.fl...  25.7 us
    unnamed x3, local copies, waits for them, and re-layouts  19.4 us
  transfers between devices with their start and end apart: 4, of which 4 were waited for; matrix products, arithmetic and copies ran while one was open for 2% of the time, Pallas kernels for 0%

commit v1 on v0

--- a/solution.py
+++ b/solution.py
@@ -9,7 +9,9 @@
 def on_device(tokens, norm_gain, up_master, down_master):
     up_local = (norm_gain[:, None] * up_master).astype(jnp.bfloat16)
     down_local = down_master.astype(jnp.bfloat16)
-    gathered = lax.all_gather(tokens, "tp", axis=1, tiled=True)
+    gathered = jnp.concatenate(
+        lax.all_to_all(jnp.stack([tokens] * lax.axis_size("tp")), "tp", 0, 0), axis=1
+    )
     widened = gathered.astype(jnp.float32)
     normed = (
         widened * lax.rsqrt(jnp.mean(widened * widened, axis=-1, keepdims=True) + norm_floor)

time: 392 us -> 356 us (0.908)
  waiting for transfers between devices: 327 us -> 236 us
  blocking collectives: 0 us -> 52.2 us
    all_gather x1, waiting for transfers between devices: 124 us -> 67.7 us  [on_device(): lax.all_gather(up_local, 'fs', axis=0, tiled=True)]
    all_to_all x0 -> x1, blocking collectives: none -> 52.2 us  [on_device(): lax.all_to_all(jnp.stack([tokens] * lax.axis_size('tp')), 'tp', 0, 0)]
    all_gather x1 -> x0, waiting for transfers between devices: 33.4 us -> none  [on_device(): gathered = lax.all_gather(tokens, 'tp', axis=1, tiled=True)]
    unnamed x3 -> x6, local copies, waits for them, and re-layouts: 19.4 us -> 20 us
  transfers between devices with their start and end apart: 4 -> 3, of which waited for: 4 -> 3; matrix products, arithmetic and copies ran while one was open for 2% -> 2% of each run, Pallas kernels for 0% -> 0%
where the time goes in v1:
time: 356 us; the launch traced here: 355 us
  waiting for transfers between devices  236 us (66%)
  blocking collectives  52.2 us (15%)
  matrix products  25.6 us (7%)
  local copies, waits for them, and re-layouts  20.5 us (6%)
  between operations  13.8 us (4%)
  other arithmetic  7.03 us (2%)
    all_gather x1, waiting for transfers between devices, on_device(): lax.all_gather(down_local, 'fs', axis=0, tiled=True)  126 us
    all_gather x1, waiting for transfers between devices, on_device(): lax.all_gather(up_local, 'fs', axis=0, tiled=True)  67.7 us
    all_to_all x1, blocking collectives, on_device(): lax.all_to_all(jnp.stack([tokens] * lax.axis_size('tp')), 'tp', 0, 0)  52.2 us
    reduce_scatter x1, waiting for transfers between devices, on_device(): lax.psum_scatter(partial_value.astype(jnp.bfloat16), 'tp', scatter_dimens...  42.7 us
    dot_general x1, matrix products, on_device(): jnp.einsum('tf,df->td', hidden, down_whole, preferred_element_type=jnp.fl...  25.6 us
    unnamed x6, local copies, waits for them, and re-layouts  20 us
  transfers between devices with their start and end apart: 3, of which 3 were waited for; matrix products, arithmetic and copies ran while one was open for 2% of the time, Pallas kernels for 0%

profile of v1, /device:TPU:0, one launch (start us, length us, event | category | flops | bytes accessed | tf_op | source)
XLA Modules:
  0.0 355.4 jit_solution(15449002225518274749)
XLA Ops:
  7.2 0.0 copy-start
  7.2 0.0 all-gather.3.cloned.1.call-start
  7.2 2.8 multiply_convert_fusion.1
  10.0 0.0 all-gather.3.cloned.1.call-update
  10.1 0.0 all-gather.5.cloned.1.call-start
  10.1 2.5 copy.8
  12.7 0.0 all-gather.5.cloned.1.call-update
  12.7 0.0 reduce-scatter.2.cloned.1.call-start
  12.7 0.0 copy-done
  12.7 0.5 copy.9
  13.3 0.5 stack.2
  13.8 52.2 %all_to_all.5 = bf16[4,1024,512]{1,2,0:T(8,128)(2,1)S(1)} all-to-all(bf16[4,1024,512]{1,2,0:T(8,128)(2,1)S(1)} %stack.2), channel_id=1, replica_groups=mesh['fs'=8,'tp'=4] {'tp'}, dimensions={0} | all-to-all | bytes 8388608 | tf_op jit(solution)/shard_map/all_to_all | solution.py:13
  66.0 0.9 multiply_reduce_fusion
  66.9 3.3 fusion
  70.2 67.7 %all-gather.3.cloned.1.call-done = bf16[2048,2048]{1,0:T(8,128)(2,1)} async-done(((bf16[256,2048]{1,0:T(8,128)(2,1)}), bf16[2048,2048]{1,0:T(8,128)(2,1)}) %all-gather.3.cloned.1.call-update) | async-done | bytes 8388624 | tf_op jit(solution)/shard_map/all_gather | solution.py:20
  137.9 125.8 %all-gather.5.cloned.1.call-done = bf16[2048,2048]{0,1:T(8,128)(2,1)} async-done(((bf16[256,2048]{0,1:T(8,128)(2,1)}), bf16[2048,2048]{0,1:T(8,128)(2,1)}) %all-gather.5.cloned.1.call-update) | async-done | bytes 8388624 | tf_op jit(solution)/shard_map/all_gather | solution.py:21
  263.7 25.6 %fusion.3 = bf16[1024,2048]{1,0:T(8,128)(2,1)} fusion(bf16[2048,2048]{0,1:T(8,128)(2,1)} %all-gather.5.cloned.1.call-done, bf16[1024,2048]{0,1:T(8,128)(2,1)} %fusion, bf16[2048,2048]{1,0:T(8,128)(2,1)} %all-gather.3.cloned.1.call-done), kind=kOutput, calls=%fused_computation.6 | convolution fusion | flops 17188257792 | bytes 25165824 | tf_op jit(solution)/shard_map/tf,df->td/dot_general | solution.py:25
  289.2 0.0 reduce-scatter.2.cloned.1.call-update
  289.3 42.7 %reduce-scatter.2.cloned.1.call-done = bf16[1024,512]{1,0:T(8,128)(2,1)} async-done(((bf16[1024,2048]{1,0:T(8,128)(2,1)}), bf16[1024,512]{1,0:T(8,128)(2,1)}) %reduce-scatter.2.cloned.1.call-update) | async-done | bytes 1048592 | tf_op jit(solution)/shard_map/reduce_scatter | solution.py:26
  332.0 8.4 %copy.12 = bf16[2048,2048]{1,0:T(8,128)(2,1)} copy(bf16[2048,2048]{1,0:T(8,128)(2,1)} %all-gather.3.cloned.1.call-done) | data formatting | bytes 16777216
  340.4 8.4 %copy.13 = bf16[2048,2048]{1,0:T(8,128)(2,1)} copy(bf16[2048,2048]{1,0:T(8,128)(2,1)} %bitcast.10) | data formatting | bytes 16777216
  (1 shorter events, 0.0 us)
Async XLA Ops:
  7.2 5.6 %copy-start = (bf16[1024,512]{1,0:T(8,128)(2,1)S(1)}, bf16[1024,512]{1,0:T(8,128)(2,1)}, u32[]{:S(2)}) copy-start(bf16[1024,512]{1,0:T(8,128)(2,1)} %param.4) | copy-start | bytes 3145732
  7.2 130.7 %all-gather.3.cloned.1.call-start = ((), (), s32[]{:S(2)}) async-start(), calls=%async_computation.2 | async-start | bytes 9437184 | tf_op jit(solution)/shard_map/all_gather | solution.py:20
  10.1 253.6 %all-gather.5.cloned.1.call-start = ((), (), s32[]{:S(2)}) async-start(), calls=%async_computation.3 | async-start | bytes 9437184 | tf_op jit(solution)/shard_map/all_gather | solution.py:21
  12.7 319.3 %reduce-scatter.2.cloned.1.call-start = ((), (), s32[]{:S(2)}) async-start(), calls=%async_computation.4 | async-start | bytes 5242880 | tf_op jit(solution)/shard_map/reduce_scatter | solution.py:26
Sparse Core Ops, SparseCore 0:
  10.7 127.1 all-gather.2
  140.5 123.1 all-gather.4
  289.4 42.5 reduce-scatter.1
